TPU v7x, 32 devices: a whole 2x2x4 slice. The times are simulated.
32 devices in a mesh: grp: 2 (over y), tp: 4 (over z), dp: 4 (over x, core).
Axes of the slice: x: 2, y: 2, z: 4, core: 2. Of those that a mesh axis runs over, the one named last changes fastest.
Arguments:
- tokens: bfloat16 [128, 4096], P('grp', 'dp'), parts along dimension 0, may hold values from -50 to 50
- lengths: int32 [128], P(('grp', 'dp')), parts along dimension 0, may hold values from 1 to 24, as said below
- norm_gain: float32 [2, 4096], P(None, 'dp'), may hold values from 0.1 to 1.9
- w_z: bfloat16 [2, 4096, 4096], P(None, 'dp', 'tp'), may hold values from -0.09375 to 0.09375
- w_x: bfloat16 [2, 4096, 4096], P(None, 'dp', 'tp'), may hold values from -0.09375 to 0.09375
- w_b: bfloat16 [2, 4096, 2048], P(None, 'dp', 'tp'), may hold values from -0.09375 to 0.09375
- w_c: bfloat16 [2, 4096, 2048], P(None, 'dp', 'tp'), may hold values from -0.09375 to 0.09375
- w_dt: bfloat16 [2, 4096, 64], P(None, 'dp'), may hold values from -0.09375 to 0.09375
- conv_weight: bfloat16 [2, 4, 8192], P(None, None, 'tp'), may hold values from -3 to 3
- dt_bias: float32 [2, 64], P(None, 'tp'), may hold values from -6 to -1.5
- a_log: float32 [2, 64], P(None, 'tp'), may hold values from 0 to 2.77
- d_skip: float32 [2, 64], P(None, 'tp'), may hold values from 0.1 to 1.9
- out_gain: float32 [2, 4096], P(None, 'tp'), may hold values from 0.1 to 1.9
- w_out: bfloat16 [2, 4096, 4096], P(None, 'tp', 'dp'), may hold values from -0.09375 to 0.09375
- conv_state: bfloat16 [2, 128, 3, 8192], P(None, ('grp', 'dp'), None, 'tp'), parts along dimension 1, may hold values from -6 to 6
- ssm_state: float32 [2, 128, 64, 64, 128], P(None, ('grp', 'dp'), 'tp'), parts along dimension 1, may hold values from -2 to 2
Outputs:
- mixed_out: bfloat16 [128, 4096], P('grp', 'dp'), parts along dimension 0
- conv_new: bfloat16 [2, 128, 3, 8192], P(None, ('grp', 'dp'), None, 'tp'), parts along dimension 1
- ssm_new: float32 [2, 128, 64, 64, 128], P(None, ('grp', 'dp'), 'tp'), parts along dimension 1
There are 2 independent parts, one for each index of `grp`. A program takes and returns all parts, laid end to end along the dimension named above; an argument that names none is the same for every part. Nothing has to cross between parts.
Inputs may be any that keep to these rules, and one draw needn't show every extreme that they name: `lengths`: each part has at least one sequence of length 24.
All inputs are finite; a program needn't handle non-finite values.
Results may differ from a plain program's by a relative error of at most 0.012.
Values may be sent and summed in bfloat16 or wider, within the bound.
A program may use at most 128 MiB of HBM per device.

v0:
```python
import jax
import jax.numpy as jnp
from jax import lax
from jax.sharding import PartitionSpec as P

D = 4096
HEADS = 64
GROUPS = 16
HEAD_DIM = 64
STATE = 128
CONV_W = 4


EPSILON = 1e-06


def body(
    tokens,
    lengths,
    norm_gain,
    w_z,
    w_x,
    w_b,
    w_c,
    w_dt,
    conv_weight,
    dt_bias,
    a_log,
    d_skip,
    out_gain,
    w_out,
    conv_state,
    ssm_state,
):
    tp_count = lax.axis_size("tp")
    local_groups = GROUPS // tp_count
    local_heads = HEADS // tp_count
    per_group = HEADS // GROUPS
    width_x = per_group * HEAD_DIM
    local_seqs = lengths.shape[0]
    offsets = jnp.arange(CONV_W - 1, dtype=jnp.int32)
    alive = lengths[:, None] + offsets[None, :] >= CONV_W
    carried = lengths >= 2
    stream = tokens
    conv_list = []
    ssm_list = []
    for layer_at in range(w_z.shape[0]):
        wide = stream.astype(jnp.float32)
        squares = jnp.sum(wide * wide, axis=-1)
        normed = (wide * norm_gain[layer_at]).astype(jnp.bfloat16)
        part_z = jnp.dot(normed, w_z[layer_at], preferred_element_type=jnp.float32)
        part_x = jnp.dot(normed, w_x[layer_at], preferred_element_type=jnp.float32)
        part_b = jnp.dot(normed, w_b[layer_at], preferred_element_type=jnp.float32)
        part_c = jnp.dot(normed, w_c[layer_at], preferred_element_type=jnp.float32)
        part_dt = jnp.dot(normed, w_dt[layer_at], preferred_element_type=jnp.float32)
        sum_z, sum_x, sum_b, sum_c, sum_dt, total_sq = (
            lax.psum_scatter(part_z, "dp", scatter_dimension=0, tiled=True),
            lax.psum_scatter(part_x, "dp", scatter_dimension=0, tiled=True),
            lax.psum_scatter(part_b, "dp", scatter_dimension=0, tiled=True),
            lax.psum_scatter(part_c, "dp", scatter_dimension=0, tiled=True),
            lax.psum_scatter(part_dt, "dp", scatter_dimension=0, tiled=True),
            lax.psum_scatter(squares, "dp", scatter_dimension=0, tiled=True),
        )
        inverse = lax.rsqrt(total_sq / D + EPSILON)[:, None]
        gating = (sum_z * inverse).astype(jnp.bfloat16)
        values = (sum_x * inverse).astype(jnp.bfloat16)
        writes = (sum_b * inverse).astype(jnp.bfloat16)
        reads = (sum_c * inverse).astype(jnp.bfloat16)
        step_all = sum_dt * inverse
        step_raw = lax.dynamic_slice_in_dim(
            step_all, lax.axis_index("tp") * local_heads, local_heads, 1
        )
        current = jnp.concatenate(
            [
                values.reshape(local_seqs, local_groups, width_x),
                writes.reshape(local_seqs, local_groups, STATE),
                reads.reshape(local_seqs, local_groups, STATE),
            ],
            axis=-1,
        ).reshape(local_seqs, local_groups * (width_x + 2 * STATE))
        conv_past = conv_state[layer_at]
        history = jnp.where(alive[:, :, None], conv_past, jnp.zeros_like(conv_past))
        conv_list.append(jnp.concatenate([history[:, 1:], current[:, None]], axis=1))
        taps_weight = conv_weight[layer_at]
        summed = current.astype(jnp.float32) * taps_weight[CONV_W - 1].astype(jnp.float32)
        for tap_at in range(CONV_W - 1):
            summed = summed + history[:, tap_at].astype(jnp.float32) * taps_weight[tap_at].astype(
                jnp.float32
            )
        activated = jax.nn.silu(summed).reshape(local_seqs, local_groups, width_x + 2 * STATE)
        head_in = activated[:, :, :width_x].reshape(local_seqs, local_groups, per_group, HEAD_DIM)
        write_keys = activated[:, :, width_x : width_x + STATE]
        read_keys = activated[:, :, width_x + STATE :]
        step = jax.nn.softplus(step_raw + dt_bias[layer_at]).reshape(
            local_seqs, local_groups, per_group
        )
        decay = jnp.exp(-jnp.exp(a_log[layer_at]).reshape(local_groups, per_group) * step)
        before = ssm_state[layer_at].reshape(local_seqs, local_groups, per_group, HEAD_DIM, STATE)
        before = jnp.where(carried[:, None, None, None, None], before, jnp.zeros_like(before))
        state_next = (
            decay[..., None, None] * before
            + (step[..., None] * head_in)[..., None] * write_keys[:, :, None, None, :]
        )
        ssm_list.append(state_next.reshape(local_seqs, local_heads, HEAD_DIM, STATE))
        readout = jnp.einsum(
            "bghpn,bgn->bghp", state_next, read_keys, precision=lax.Precision.HIGHEST
        )
        readout = readout + d_skip[layer_at].reshape(local_groups, per_group)[..., None] * head_in
        gated = readout.reshape(local_seqs, local_groups, width_x) * jax.nn.silu(
            gating.astype(jnp.float32).reshape(local_seqs, local_groups, width_x)
        )
        gated = (
            gated
            * lax.rsqrt(jnp.mean(gated * gated, axis=-1, keepdims=True) + EPSILON)
            * out_gain[layer_at].reshape(local_groups, width_x)
        )
        mixed = gated.reshape(local_seqs, local_heads * HEAD_DIM).astype(jnp.bfloat16)
        out_weight = w_out[layer_at]

        def project(section, offset, weight=out_weight):
            return jnp.dot(section, weight, preferred_element_type=jnp.float32)

        partial_value = project(lax.all_gather(mixed, "dp", axis=0, tiled=True), jnp.int32(0))
        share = lax.psum_scatter(partial_value, "tp", scatter_dimension=0, tiled=True)
        share_rows = share.shape[0]
        own_rows = lax.dynamic_slice_in_dim(wide, lax.axis_index("tp") * share_rows, share_rows, 0)
        stream = lax.all_gather((own_rows + share).astype(jnp.bfloat16), "tp", axis=0, tiled=True)
    return (stream, jnp.stack(conv_list), jnp.stack(ssm_list))


def solution(mesh):
    placed = (
        P("grp", "dp"),
        P(("grp", "dp")),
        P(None, "dp"),
        P(None, "dp", "tp"),
        P(None, "dp", "tp"),
        P(None, "dp", "tp"),
        P(None, "dp", "tp"),
        P(None, "dp", None),
        P(None, None, "tp"),
        P(None, "tp"),
        P(None, "tp"),
        P(None, "tp"),
        P(None, "tp"),
        P(None, "tp", "dp"),
        P(None, ("grp", "dp"), None, "tp"),
        P(None, ("grp", "dp"), "tp", None, None),
    )
    return jax.shard_map(
        body,
        mesh=mesh,
        in_specs=placed,
        out_specs=(
            P("grp", "dp"),
            P(None, ("grp", "dp"), None, "tp"),
            P(None, ("grp", "dp"), "tp", None, None),
        ),
        check_vma=False,
    )
```

profile of v0, /device:TPU:0, one launch (start us, length us, event | category | flops | bytes accessed | tf_op | source)
XLA Modules:
  0.0 389.5 jit_solution(12363132450927614459)
XLA Ops:
  8.1 1.7 fusion.56
  9.9 2.2 fusion.42
  12.2 2.3 fusion.44
  14.5 2.9 fusion.30
  17.5 2.9 fusion.28
  20.6 8.4 %all-reduce = f32[64]{0:T(128)S(1)} all-reduce(f32[64]{0:T(128)S(1)} %multiply_reduce_fusion.1), channel_id=3, replica_groups=mesh['grp'=2,'tp'=4,'dp'=4] {'dp'}, use_global_device_ids=true, to_apply=%region_2.0.clone | all-reduce | flops 64 | bytes 512
  29.7 8.5 %slice.166 = f32[1,16,16,64,128]{4,3,2,1,0:T(8,128)} slice(f32[2,16,16,64,128]{4,3,2,1,0:T(8,128)} %param.31), slice={[0:1], [0:16], [0:16], [0:64], [0:128]} | slice | bytes 16777216 | tf_op jit(solution)/shard_map/slice | solution.py:98
  40.9 14.5 %reduce-scatter.19.cloned.1.call-done = f32[16,512]{1,0:T(8,128)} async-done(((f32[64,512]{1,0:T(8,128)}), f32[16,512]{1,0:T(8,128)}) %reduce-scatter.19.cloned.1.call-update) | async-done | bytes 32784 | tf_op jit(solution)/shard_map/reduce_scatter | solution.py:60
  55.4 22.1 %reduce-scatter.17.cloned.1.call-done = f32[16,512]{1,0:T(8,128)} async-done(((f32[64,512]{1,0:T(8,128)}), f32[16,512]{1,0:T(8,128)}) %reduce-scatter.17.cloned.1.call-update) | async-done | bytes 32784 | tf_op jit(solution)/shard_map/reduce_scatter | solution.py:59
  78.4 22.1 %reduce-scatter.15.cloned.1.call-done = f32[16,1024]{1,0:T(8,128)} async-done(((f32[64,1024]{1,0:T(8,128)}), f32[16,1024]{1,0:T(8,128)}) %reduce-scatter.15.cloned.1.call-update) | async-done | bytes 65552 | tf_op jit(solution)/shard_map/reduce_scatter | solution.py:58
  100.5 22.4 %reduce-scatter.21.cloned.1.call-done = f32[16,1024]{1,0:T(8,128)} async-done(((f32[64,1024]{1,0:T(8,128)}), f32[16,1024]{1,0:T(8,128)}) %reduce-scatter.21.cloned.1.call-update) | async-done | bytes 65552 | tf_op jit(solution)/shard_map/reduce_scatter | solution.py:57
  124.5 22.0 %fusion.5 = f32[16,4,1,4,64]{4,2,3,1,0:T(1,128)S(1)} fusion(f32[16,4,128,1,1]{2,3,4,1,0:T(1,128)S(1)} %bitcast.108, f32[16,4,4,64,128]{4,3,2,1,0:T(8,128)} %bitcast.93, f32[16,4,128]{2,1,0:T(4,128)S(1)} %get-tuple-element.36, f32[16,4,4,64]{3,2,1,0:T(4,128)S(1)} %broadcast_multiply_fusion.3, f32[16,4,4]{2,1,0:T(4,128)S(1)} %copy.26, ...), kind=kOutput, calls=%fused_computation.8 | convolution fusion | flops 33554432 | bytes 8586256 | tf_op jit(solution)/shard_map/bghpn,bgn->bghp/dot_general | solution.py:105
  147.0 5.4 %all_gather.12 = bf16[64,1024]{1,0:T(8,128)(2,1)S(1)} all-gather(bf16[16,1024]{1,0:T(8,128)(2,1)S(1)} %multiply_convert_fusion.5), channel_id=1, replica_groups=mesh['grp'=2,'tp'=4,'dp'=4] {'dp'}, dimensions={0}, use_global_device_ids=true | all-gather | bytes 163840 | tf_op jit(solution)/shard_map/all_gather | solution.py:123
  152.5 2.8 fusion.26
  156.0 19.4 %reduce-scatter.23.cloned.1.call-done = f32[16,1024]{1,0:T(8,128)} async-done(((f32[64,1024]{1,0:T(8,128)}), f32[16,1024]{1,0:T(8,128)}) %reduce-scatter.23.cloned.1.call-update) | async-done | bytes 65552 | tf_op jit(solution)/shard_map/reduce_scatter | solution.py:124
  176.3 13.4 %all_gather.13 = bf16[64,1024]{1,0:T(8,128)(2,1)S(1)} all-gather(bf16[16,1024]{1,0:T(8,128)(2,1)S(1)} %add_convert_fusion.1), channel_id=1, replica_groups=mesh['grp'=2,'tp'=4,'dp'=4] {'tp'}, dimensions={0}, use_global_device_ids=true | all-gather | bytes 163840 | tf_op jit(solution)/shard_map/all_gather | solution.py:127
  190.5 2.2 fusion.38
  192.9 2.2 fusion.40
  195.2 2.8 fusion.24
  198.2 5.7 %all-reduce.1 = f32[64]{0:T(128)S(1)} all-reduce(f32[64]{0:T(128)S(1)} %multiply_reduce_fusion), channel_id=10, replica_groups=mesh['grp'=2,'tp'=4,'dp'=4] {'dp'}, use_global_device_ids=true, to_apply=%region_11.12.clone | all-reduce | flops 64 | bytes 512
  203.9 2.8 fusion.22
  209.5 21.5 %reduce-scatter.31.cloned.1.call-done = f32[16,512]{1,0:T(8,128)} async-done(((f32[64,512]{1,0:T(8,128)}), f32[16,512]{1,0:T(8,128)}) %reduce-scatter.31.cloned.1.call-update) | async-done | bytes 32784 | tf_op jit(solution)/shard_map/reduce_scatter | solution.py:60
  231.0 22.1 %reduce-scatter.29.cloned.1.call-done = f32[16,512]{1,0:T(8,128)} async-done(((f32[64,512]{1,0:T(8,128)}), f32[16,512]{1,0:T(8,128)}) %reduce-scatter.29.cloned.1.call-update) | async-done | bytes 32784 | tf_op jit(solution)/shard_map/reduce_scatter | solution.py:59
  254.0 22.0 %reduce-scatter.27.cloned.1.call-done = f32[16,1024]{1,0:T(8,128)} async-done(((f32[64,1024]{1,0:T(8,128)}), f32[16,1024]{1,0:T(8,128)}) %reduce-scatter.27.cloned.1.call-update) | async-done | bytes 65552 | tf_op jit(solution)/shard_map/reduce_scatter | solution.py:58
  276.0 23.1 %reduce-scatter.33.cloned.1.call-done = f32[16,1024]{1,0:T(8,128)} async-done(((f32[64,1024]{1,0:T(8,128)}), f32[16,1024]{1,0:T(8,128)}) %reduce-scatter.33.cloned.1.call-update) | async-done | bytes 65552 | tf_op jit(solution)/shard_map/reduce_scatter | solution.py:57
  301.1 16.4 %multiply_add_fusion.1 = (f32[1,16,16,64,128]{4,3,2,1,0:T(8,128)}, f32[1,16,16,64,128]{4,3,2,1,0:T(8,128)}, f32[1,16,16,64,128]{4,3,2,1,0:T(8,128)S(1)}) fusion(f32[16,16,128]{2,1,0:T(8,128)S(1)} %bitcast.95, f32[16,16,64]{2,1,0:T(8,128)S(1)} %broadcast_multiply_fusion.1, f32[16,16]{1,0:T(8,128)S(1)} %get-tuple-element.15, ...), kind=kLoop, calls=%fused_computation.2 | loop fusion | flops 16777216 | bytes 42338320 | tf_op jit(solution)/shard_map/add | solution.py:101
  317.5 21.2 %fusion = f32[16,4,1,4,64]{4,2,3,1,0:T(1,128)S(1)} fusion(f32[16,4,128,1,1]{2,3,4,1,0:T(1,128)S(1)} %bitcast.107, f32[16,4,4,64,128]{4,3,2,1,0:T(8,128)S(1)} %bitcast.94, f32[16,4,128]{2,1,0:T(4,128)S(1)} %get-tuple-element.34, f32[16,4,4,64]{3,2,1,0:T(4,128)S(1)} %broadcast_multiply_fusion.2, f32[16,4,4]{2,1,0:T(4,128)S(1)} %copy.29, ...), kind=kOutput, calls=%fused_computation.3 | convolution fusion | flops 33554432 | bytes 8586256 | tf_op jit(solution)/shard_map/bghpn,bgn->bghp/dot_general | solution.py:105
  339.4 5.4 %all_gather.14 = bf16[64,1024]{1,0:T(8,128)(2,1)S(1)} all-gather(bf16[16,1024]{1,0:T(8,128)(2,1)S(1)} %multiply_convert_fusion.2), channel_id=1, replica_groups=mesh['grp'=2,'tp'=4,'dp'=4] {'dp'}, dimensions={0}, use_global_device_ids=true | all-gather | bytes 163840 | tf_op jit(solution)/shard_map/all_gather | solution.py:123
  344.8 2.8 fusion.20
  348.4 12.0 %pad_maximum_fusion = f32[2,16,16,64,128]{4,3,2,1,0:T(8,128)} fusion(f32[1,16,16,64,128]{4,3,2,1,0:T(8,128)} %get-tuple-element.24, f32[1,16,16,64,128]{4,3,2,1,0:T(8,128)} %get-tuple-element.23), kind=kLoop, calls=%fused_computation | loop fusion | flops 4194304 | bytes 33554432 | tf_op jit(solution)/shard_map/stack | solution.py:128
  360.4 7.4 %reduce-scatter.35.cloned.1.call-done = f32[16,1024]{1,0:T(8,128)} async-done(((f32[64,1024]{1,0:T(8,128)}), f32[16,1024]{1,0:T(8,128)}) %reduce-scatter.35.cloned.1.call-update) | async-done | bytes 65552 | tf_op jit(solution)/shard_map/reduce_scatter | solution.py:124
  368.6 13.4 %all_gather.15 = bf16[64,1024]{1,0:T(8,128)(2,1)S(1)} all-gather(bf16[16,1024]{1,0:T(8,128)(2,1)S(1)} %add_convert_fusion), channel_id=1, replica_groups=mesh['grp'=2,'tp'=4,'dp'=4] {'tp'}, dimensions={0}, use_global_device_ids=true | all-gather | bytes 163840 | tf_op jit(solution)/shard_map/all_gather | solution.py:127
  (148 shorter events, 18.3 us)
Async XLA Ops:
  7.2 13.2 %copy-start = (bf16[64,1024]{1,0:T(8,128)(2,1)S(1)}, bf16[64,1024]{1,0:T(8,128)(2,1)}, u32[]{:S(2)}) copy-start(bf16[64,1024]{1,0:T(8,128)(2,1)} %param.16) | copy-start | bytes 393220
  7.2 13.4 %copy-start.8 = (s32[16]{0:T(128)S(1)}, s32[16]{0:T(128)}, u32[]{:S(2)}) copy-start(s32[16]{0:T(128)} %param.17) | copy-start | bytes 196
  7.2 21.8 %copy-start.1 = (bf16[2,16,3,2048]{3,1,2,0:T(8,128)(2,1)S(1)}, bf16[2,16,3,2048]{3,1,2,0:T(8,128)(2,1)}, u32[]{:S(2)}) copy-start(bf16[2,16,3,2048]{3,1,2,0:T(8,128)(2,1)} %param.30) | copy-start | bytes 1179652
  7.2 22.2 %copy-start.2 = (bf16[2,4,2048]{2,1,0:T(4,128)(2,1)S(1)}, bf16[2,4,2048]{2,1,0:T(4,128)(2,1)}, u32[]{:S(2)}) copy-start(bf16[2,4,2048]{2,1,0:T(4,128)(2,1)} %param.24) | copy-start | bytes 98308
  7.2 32.5 %reduce-scatter.13.cloned.1.call-start = ((), (), s32[]{:S(2)}) async-start(), calls=%async_computation.12 | async-start | bytes 40960 | tf_op jit(solution)/shard_map/reduce_scatter | solution.py:61
  9.8 45.5 %reduce-scatter.19.cloned.1.call-start = ((), (), s32[]{:S(2)}) async-start(), calls=%async_computation.15 | async-start | bytes 163840 | tf_op jit(solution)/shard_map/reduce_scatter | solution.py:60
  12.2 65.3 %reduce-scatter.17.cloned.1.call-start = ((), (), s32[]{:S(2)}) async-start(), calls=%async_computation.14 | async-start | bytes 163840 | tf_op jit(solution)/shard_map/reduce_scatter | solution.py:59
  14.5 86.0 %reduce-scatter.15.cloned.1.call-start = ((), (), s32[]{:S(2)}) async-start(), calls=%async_computation.13 | async-start | bytes 327680 | tf_op jit(solution)/shard_map/reduce_scatter | solution.py:58
  17.4 105.4 %reduce-scatter.21.cloned.1.call-start = ((), (), s32[]{:S(2)}) async-start(), calls=%async_computation.16 | async-start | bytes 327680 | tf_op jit(solution)/shard_map/reduce_scatter | solution.py:57
  20.3 155.1 %reduce-scatter.23.cloned.1.call-start = ((), (), s32[]{:S(2)}) async-start(), calls=%async_computation.17 | async-start | bytes 327680 | tf_op jit(solution)/shard_map/reduce_scatter | solution.py:124
  29.7 8.5 %copy-start.4 = (f32[2,16]{1,0:T(2,128)S(1)}, f32[2,16]{1,0:T(2,128)}, u32[]{:S(2)}) copy-start(f32[2,16]{1,0:T(2,128)} %param.26) | copy-start | bytes 388
  29.7 8.6 %copy-start.5 = (f32[2,16]{1,0:T(2,128)S(1)}, f32[2,16]{1,0:T(2,128)}, u32[]{:S(2)}) copy-start(f32[2,16]{1,0:T(2,128)} %param.25) | copy-start | bytes 388
  29.7 8.7 %copy-start.6 = (f32[2,16]{1,0:T(2,128)S(1)}, f32[2,16]{1,0:T(2,128)}, u32[]{:S(2)}) copy-start(f32[2,16]{1,0:T(2,128)} %param.27) | copy-start | bytes 388
  29.7 8.7 %copy-start.3 = (f32[2,1024]{1,0:T(2,128)S(1)}, f32[2,1024]{1,0:T(2,128)}, u32[]{:S(2)}) copy-start(f32[2,1024]{1,0:T(2,128)} %param.28) | copy-start | bytes 24580
  29.7 8.8 %copy-start.9 = (u32[32]{0:T(128)S(1)}, u32[32]{0:T(128)}, u32[]{:S(2)}) copy-start(u32[32]{0:T(128)} %constant.43) | copy-start | bytes 388
  124.5 65.2 %copy-start.7 = (bf16[2,1024,64]{1,2,0:T(8,128)(2,1)S(1)}, bf16[2,1024,64]{1,2,0:T(8,128)(2,1)}, u32[]{:S(2)}) copy-start(bf16[2,1024,64]{1,2,0:T(8,128)(2,1)} %param.23) | copy-start | bytes 786436
  155.3 53.1 %reduce-scatter.25.cloned.1.call-start = ((), (), s32[]{:S(2)}) async-start(), calls=%async_computation.18 | async-start | bytes 40960 | tf_op jit(solution)/shard_map/reduce_scatter | solution.py:61
  190.5 40.5 %reduce-scatter.31.cloned.1.call-start = ((), (), s32[]{:S(2)}) async-start(), calls=%async_computation.21 | async-start | bytes 163840 | tf_op jit(solution)/shard_map/reduce_scatter | solution.py:60
  192.7 60.4 %reduce-scatter.29.cloned.1.call-start = ((), (), s32[]{:S(2)}) async-start(), calls=%async_computation.20 | async-start | bytes 163840 | tf_op jit(solution)/shard_map/reduce_scatter | solution.py:59
  195.1 80.9 %reduce-scatter.27.cloned.1.call-start = ((), (), s32[]{:S(2)}) async-start(), calls=%async_computation.19 | async-start | bytes 327680 | tf_op jit(solution)/shard_map/reduce_scatter | solution.py:58
  198.0 101.2 %reduce-scatter.33.cloned.1.call-start = ((), (), s32[]{:S(2)}) async-start(), calls=%async_computation.22 | async-start | bytes 327680 | tf_op jit(solution)/shard_map/reduce_scatter | solution.py:57
  206.8 161.0 %reduce-scatter.35.cloned.1.call-start = ((), (), s32[]{:S(2)}) async-start(), calls=%async_computation.23 | async-start | bytes 327680 | tf_op jit(solution)/shard_map/reduce_scatter | solution.py:124
Sparse Core Ops, SparseCore 0:
  10.4 22.2 reduce-scatter.12
  35.7 19.6 reduce-scatter.18
  57.8 19.6 reduce-scatter.16
  80.4 20.0 reduce-scatter.14
  102.8 20.0 reduce-scatter.20
  155.4 19.9 reduce-scatter.22
  190.6 17.6 reduce-scatter.24
  211.3 19.6 reduce-scatter.30
  233.4 19.6 reduce-scatter.28
  256.0 19.9 reduce-scatter.26
  279.1 20.0 reduce-scatter.32
  347.7 20.0 reduce-scatter.34
where the time goes:
time: 391 us; the launch traced here: 389 us
  waiting for transfers between devices  198 us (51%)
  matrix products  71.4 us (18%)
  blocking collectives  51.6 us (13%)
  other arithmetic  38.5 us (10%)
  between operations  15.3 us (4%)
  local copies, waits for them, and re-layouts  13.7 us (4%)
    reduce_scatter x2, waiting for transfers between devices, body(): lax.psum_scatter(part_z, 'dp', scatter_dimension=0, tiled=True)  45.5 us
    reduce_scatter x2, waiting for transfers between devices, body(): lax.psum_scatter(part_b, 'dp', scatter_dimension=0, tiled=True)  44.2 us
    reduce_scatter x2, waiting for transfers between devices, body(): lax.psum_scatter(part_x, 'dp', scatter_dimension=0, tiled=True)  44.1 us
    dot_general x2, matrix products, body(): jnp.einsum('bghpn,bgn->bghp', state_next, read_keys, precision=lax.Precis...  43.2 us
    reduce_scatter x2, waiting for transfers between devices, body(): lax.psum_scatter(part_c, 'dp', scatter_dimension=0, tiled=True)  36 us
    reduce_scatter x2, waiting for transfers between devices, body(): lax.psum_scatter(partial_value, 'tp', scatter_dimension=0, tiled=True)  26.8 us
    all_gather x2, blocking collectives, body(): lax.all_gather((own_rows + share).astype(jnp.bfloat16), 'tp', axis=0, til...  26.7 us
    add x1, other arithmetic, body(): decay[..., None, None] * before  16.4 us
  transfers between devices with their start and end apart: 12, of which 11 were waited for; matrix products, arithmetic and copies ran while one was open for 12% of the time, Pallas kernels for 0%

commit v1 on v0

v1 whole, which is shorter than its diff:
```python
import functools

import jax
import jax.numpy as jnp
from jax import lax
from jax.experimental import pallas as pl
from jax.experimental.pallas import tpu as pltpu
from jax.sharding import PartitionSpec as P

D = 4096
HEADS = 64
GROUPS = 16
HEAD_DIM = 64
STATE = 128
CONV_W = 4
PER_GROUP = HEADS // GROUPS
WIDTH_X = PER_GROUP * HEAD_DIM
GROUP_W = WIDTH_X + 2 * STATE
EPSILON = 1e-06
MESH = pl.DeviceIdType.MESH
BF16 = jnp.bfloat16
F32 = jnp.float32


def silu(t):
    return t / (1.0 + jnp.exp(-t))


def block_kernel(
    nd, nt,
    tokens_ref, lens_ref, gain_ref, bias_ref, alog_ref, skip_ref, ogain_ref, taps_ref, conv_ref,
    wz_hbm, wx_hbm, wb_hbm, wc_hbm, wdt_hbm, wo_hbm, state_hbm,
    out_ref, cur_ref, dec_ref, sx_ref, wk_ref,
    wz, wx, wb, wc, wdt, wo, state,
    snd_e, snd_x, snd_b, snd_c, snd_z,
    rcv_e, rcv_x, rcv_b, rcv_c, rcv_z,
    mixes, snd_o, rcv_o, stream, normed_s, rk_s, y_s,
    w_sem, st_sem, dps, dpr, ags, agr, rss, rsr, tgs, tgr,
):
    dp = lax.axis_index("dp")
    tp = lax.axis_index("tp")
    layers = gain_ref.shape[0]
    seqs = lens_ref.shape[0]
    batch = nd * seqs
    rows = batch // nt
    dloc = gain_ref.shape[1]
    width = wx.shape[2]
    lgroups = width // WIDTH_X

    pairs = ((wdt_hbm, wdt), (wx_hbm, wx), (wb_hbm, wb), (wc_hbm, wc), (wz_hbm, wz), (wo_hbm, wo))

    def weight(layer, at):
        src, dst = pairs[at]
        return pltpu.make_async_copy(src.at[layer], dst.at[layer], w_sem.at[layer, at])

    def states(layer):
        return pltpu.make_async_copy(state_hbm.at[layer], state.at[layer], st_sem.at[layer])

    for at in range(5):
        weight(0, at).start()

    barrier = pltpu.get_barrier_semaphore()
    for k in range(1, nd):
        pl.semaphore_signal(
            barrier, inc=1, device_id={"dp": lax.rem(dp + k, nd)}, device_id_type=MESH
        )
    for k in range(1, nt):
        pl.semaphore_signal(
            barrier, inc=1, device_id={"tp": lax.rem(tp + k, nt)}, device_id_type=MESH
        )
    pl.semaphore_wait(barrier, nd - 1 + nt - 1)

    def scatter(layer, snd, rcv, at):
        copies = []
        for k in range(1, nd):
            peer = lax.rem(dp + k, nd)
            copy = pltpu.make_async_remote_copy(
                src_ref=snd.at[layer, peer],
                dst_ref=rcv.at[layer, k - 1],
                send_sem=dps.at[layer, at, k - 1],
                recv_sem=dpr.at[layer, at, k - 1],
                device_id={"dp": peer},
                device_id_type=MESH,
            )
            copy.start()
            copies.append(copy)
        return copies

    def gathered(copies, layer, snd, rcv):
        for copy in copies:
            copy.wait_recv()
        total = snd[layer, dp].astype(F32)
        for k in range(nd - 1):
            total = total + rcv[layer, k].astype(F32)
        return total

    heads_all = wdt.shape[2]
    lheads = bias_ref.shape[1]

    def expand(values, offset):
        count = values.shape[1]
        head = lax.broadcasted_iota(jnp.int32, (count, width), 0)
        lane = lax.broadcasted_iota(jnp.int32, (count, width), 1)
        pick = jnp.where(head == lane // HEAD_DIM + offset, 1.0, 0.0).astype(F32)
        return jnp.dot(
            values, pick, preferred_element_type=F32, precision=lax.Precision.HIGHEST
        )

    bias = expand(bias_ref[...], 0)
    rate = jnp.exp(expand(alog_ref[...], 0))
    skip = expand(skip_ref[...], 0)
    lens = lens_ref[...]
    pending = []

    for layer in range(layers):
        source = tokens_ref if layer == 0 else stream.at[layer - 1]
        wide = source[...].astype(F32).reshape(batch, dloc)
        squares = jnp.sum(wide * wide, axis=-1, keepdims=True)
        normed_s[...] = (wide * gain_ref[layer : layer + 1, :]).astype(BF16)

        def project(w_ref, snd, layer=layer):
            n = w_ref.shape[2]
            tile = min(n, 256)

            def step(j, carry):
                cols = pl.ds(pl.multiple_of(j * tile, tile), tile)
                part = jnp.dot(
                    normed_s[...], w_ref[layer, :, cols], preferred_element_type=F32
                )
                snd[layer, :, :, cols] = part.reshape(nd, seqs, tile).astype(snd.dtype)
                return carry

            lax.fori_loop(0, n // tile, step, 0)

        weight(layer, 0).wait()
        part_dt = jnp.dot(normed_s[...], wdt[layer], preferred_element_type=F32)
        snd_e[layer, :, :, 0:128] = jnp.zeros((nd, seqs, 128), F32)
        snd_e[layer, :, :, 0:heads_all] = part_dt.reshape(nd, seqs, heads_all)
        snd_e[layer, :, :, 128:256] = jnp.broadcast_to(squares, (batch, 128)).reshape(
            nd, seqs, 128
        )
        weight(layer, 1).wait()
        project(wx, snd_x)
        copies_x = scatter(layer, snd_x, rcv_x, 1)
        copies_e = scatter(layer, snd_e, rcv_e, 0)
        weight(layer, 2).wait()
        project(wb, snd_b)
        copies_b = scatter(layer, snd_b, rcv_b, 2)
        weight(layer, 3).wait()
        project(wc, snd_c)
        copies_c = scatter(layer, snd_c, rcv_c, 3)
        weight(layer, 4).wait()
        if layer == 0:
            states(0).start()
            weight(0, 5).start()
        project(wz, snd_z)
        copies_z = scatter(layer, snd_z, rcv_z, 4)
        if layer + 1 < layers:
            for at in range(6):
                weight(layer + 1, at).start()
            states(layer + 1).start()

        extra = gathered(copies_e, layer, snd_e, rcv_e)
        inverse = lax.rsqrt(extra[:, 128:129] / D + EPSILON)
        raw = expand(extra[:, 0:heads_all] * inverse, tp * lheads)
        softin = raw + bias[layer : layer + 1, :]
        step = jnp.maximum(softin, 0.0) + jnp.log1p(jnp.exp(-jnp.abs(softin)))
        decay = jnp.exp(-rate[layer : layer + 1, :] * step)
        decay = jnp.where(lens >= 2, decay, 0.0)

        values = (gathered(copies_x, layer, snd_x, rcv_x) * inverse).astype(BF16)
        writes = (gathered(copies_b, layer, snd_b, rcv_b) * inverse).astype(BF16)
        reads = (gathered(copies_c, layer, snd_c, rcv_c) * inverse).astype(BF16)
        pieces = []
        for g in range(lgroups):
            pieces.append(values[:, g * WIDTH_X : (g + 1) * WIDTH_X])
            pieces.append(writes[:, g * STATE : (g + 1) * STATE])
            pieces.append(reads[:, g * STATE : (g + 1) * STATE])
        current = jnp.concatenate(pieces, axis=1)
        cur_ref[layer] = current
        conv_w = lgroups * GROUP_W
        summed = current.astype(F32) * taps_ref[
            layer, CONV_W - 1 : CONV_W, :
        ].astype(F32)
        for tap in range(CONV_W - 1):
            past = conv_ref[layer, :, tap * conv_w : (tap + 1) * conv_w].astype(F32)
            past = jnp.where(lens + tap >= CONV_W, past, 0.0)
            summed = summed + past * taps_ref[layer, tap : tap + 1, :].astype(F32)
        active = silu(summed)
        head_in = jnp.concatenate(
            [active[:, g * GROUP_W : g * GROUP_W + WIDTH_X] for g in range(lgroups)], axis=1
        )
        wk = [
            active[:, g * GROUP_W + WIDTH_X : g * GROUP_W + WIDTH_X + STATE]
            for g in range(lgroups)
        ]
        rk = [active[:, g * GROUP_W + WIDTH_X + STATE : (g + 1) * GROUP_W] for g in range(lgroups)]
        stepx = step * head_in
        dec_ref[layer] = decay
        sx_ref[layer] = stepx
        wk_ref[layer] = jnp.concatenate(wk, axis=1)
        rk_s[...] = jnp.concatenate(rk, axis=1)

        states(layer).wait()

        def read_eight(b, carry, layer=layer):
            at = pl.ds(pl.multiple_of(b * 8, 8), 8)
            keys = rk_s[at, :]
            lines = []
            for i in range(8):
                outs = []
                for g in range(lgroups):
                    row = keys[i : i + 1, g * STATE : (g + 1) * STATE]
                    lhs = jnp.broadcast_to(row, (16, STATE)).astype(BF16)
                    held = state[layer, b * 8 + i, g * PER_GROUP : (g + 1) * PER_GROUP]
                    held = held.reshape(WIDTH_X, STATE).astype(BF16)
                    res = lax.dot_general(
                        lhs, held, (((1,), (1,)), ((), ())), preferred_element_type=F32
                    )
                    outs.append(res[0:1])
                lines.append(jnp.concatenate(outs, axis=1))
            y_s[at, :] = jnp.concatenate(lines, axis=0)
            return carry

        lax.fori_loop(0, seqs // 8, read_eight, 0)
        readout = decay * y_s[...] + skip[layer : layer + 1, :] * head_in
        gate = (gathered(copies_z, layer, snd_z, rcv_z) * inverse).astype(BF16).astype(F32)
        gate = silu(gate)
        mixed = []
        for g in range(lgroups):
            cols = slice(g * WIDTH_X, (g + 1) * WIDTH_X)
            cross = jnp.sum(wk[g] * rk[g], axis=-1, keepdims=True)
            gated = (readout[:, cols] + stepx[:, cols] * cross) * gate[:, cols]
            norm = lax.rsqrt(jnp.mean(gated * gated, axis=-1, keepdims=True) + EPSILON)
            mixed.append(gated * norm * ogain_ref[layer : layer + 1, cols])
        mixes[layer, dp] = jnp.concatenate(mixed, axis=1).astype(BF16)
        copies_m = []
        for k in range(1, nd):
            copy = pltpu.make_async_remote_copy(
                src_ref=mixes.at[layer, dp],
                dst_ref=mixes.at[layer, dp],
                send_sem=ags.at[layer, k - 1],
                recv_sem=agr.at[layer, k - 1],
                device_id={"dp": lax.rem(dp + k, nd)},
                device_id_type=MESH,
            )
            copy.start()
            copies_m.append(copy)
        weight(layer, 5).wait()
        for copy in copies_m:
            copy.wait_recv()

        tile = min(dloc, 256)

        def project_out(j, carry, layer=layer):
            cols = pl.ds(pl.multiple_of(j * tile, tile), tile)
            lhs = mixes[layer].reshape(batch, width)
            part = jnp.dot(lhs, wo[layer, :, cols], preferred_element_type=F32)
            snd_o[layer, :, :, cols] = part.reshape(nt, rows, tile).astype(BF16)
            return carry

        lax.fori_loop(0, dloc // tile, project_out, 0)
        copies_o = []
        for k in range(1, nt):
            peer = lax.rem(tp + k, nt)
            copy = pltpu.make_async_remote_copy(
                src_ref=snd_o.at[layer, peer],
                dst_ref=rcv_o.at[layer, k - 1],
                send_sem=rss.at[layer, k - 1],
                recv_sem=rsr.at[layer, k - 1],
                device_id={"tp": peer},
                device_id_type=MESH,
            )
            copy.start()
            copies_o.append(copy)
        total = source[tp].astype(F32) + snd_o[layer, tp].astype(F32)
        for k in range(nt - 1):
            copies_o[k].wait_recv()
            total = total + rcv_o[layer, k].astype(F32)
        stream[layer, tp] = total.astype(BF16)
        copies_s = []
        for k in range(1, nt):
            copy = pltpu.make_async_remote_copy(
                src_ref=stream.at[layer, tp],
                dst_ref=stream.at[layer, tp],
                send_sem=tgs.at[layer, k - 1],
                recv_sem=tgr.at[layer, k - 1],
                device_id={"tp": lax.rem(tp + k, nt)},
                device_id_type=MESH,
            )
            copy.start()
            copies_s.append(copy)
        for copy in copies_s:
            copy.wait_recv()
        for group in (copies_e, copies_x, copies_b, copies_c, copies_z, copies_m, copies_o, copies_s):
            pending.extend(group)

    out_ref[...] = stream[layers - 1]
    for copy in pending:
        copy.wait_send()


def state_kernel(dec_ref, sx_ref, wk_ref, state_ref, new_ref):
    count = state_ref.shape[1]
    first = pl.program_id(1) * count
    width = dec_ref.shape[2]
    at = pl.ds(pl.multiple_of(first // 8 * 8, 8), 8)
    layer = pl.program_id(0)
    place = lax.rem(first, 8)

    def rows_of(ref):
        block = ref[layer, at, :]
        rows = block[0:count]
        for j in range(count, 8, count):
            rows = jnp.where(place == j, block[j : j + count], rows)
        return rows

    decs, sxs, wks = rows_of(dec_ref), rows_of(sx_ref), rows_of(wk_ref)
    for i in range(count):
        dec = jnp.broadcast_to(decs[i : i + 1], (64, width))
        sx = jnp.broadcast_to(sxs[i : i + 1], (64, width))
        cols = jnp.concatenate([dec, sx], axis=0).T
        for g in range(width // WIDTH_X):
            part = cols[g * WIDTH_X : (g + 1) * WIDTH_X]
            held = state_ref[0, i, g * PER_GROUP : (g + 1) * PER_GROUP].reshape(WIDTH_X, STATE)
            write = wks[i : i + 1, g * STATE : (g + 1) * STATE]
            new = part[:, 0:1] * held + part[:, 64:65] * write
            new_ref[0, i, g * PER_GROUP : (g + 1) * PER_GROUP] = new.reshape(
                PER_GROUP, HEAD_DIM, STATE
            )


def body(
    nd, nt,
    tokens, lengths, norm_gain, w_z, w_x, w_b, w_c, w_dt, conv_weight,
    dt_bias, a_log, d_skip, out_gain, w_out, conv_state, ssm_state,
):
    layers = w_z.shape[0]
    batch, dloc = tokens.shape
    seqs = lengths.shape[0]
    rows = batch // nt
    width = w_x.shape[2]
    keys = w_b.shape[2]
    heads_all = w_dt.shape[2]
    conv_w = conv_weight.shape[2]
    vmem = pl.BlockSpec(memory_space=pltpu.VMEM)
    anywhere = pl.BlockSpec(memory_space=pl.ANY)
    dma = pltpu.SemaphoreType.DMA
    sizes = (width, keys, keys, width)
    stream, current, dec, sx, wk = pl.pallas_call(
        functools.partial(block_kernel, nd, nt),
        out_shape=(
            jax.ShapeDtypeStruct((nt, rows, dloc), BF16),
            jax.ShapeDtypeStruct((layers, seqs, conv_w), BF16),
            jax.ShapeDtypeStruct((layers, seqs, width), F32),
            jax.ShapeDtypeStruct((layers, seqs, width), F32),
            jax.ShapeDtypeStruct((layers, seqs, keys), F32),
        ),
        in_specs=[vmem] * 9 + [anywhere] * 7,
        out_specs=[vmem] * 5,
        scratch_shapes=[
            pltpu.VMEM(w_z.shape, BF16),
            pltpu.VMEM(w_x.shape, BF16),
            pltpu.VMEM(w_b.shape, BF16),
            pltpu.VMEM(w_c.shape, BF16),
            pltpu.VMEM(w_dt.shape, BF16),
            pltpu.VMEM(w_out.shape, BF16),
            pltpu.VMEM(ssm_state.shape, F32),
            pltpu.VMEM((layers, nd, seqs, 256), F32),
            *[pltpu.VMEM((layers, nd, seqs, n), BF16) for n in sizes],
            pltpu.VMEM((layers, nd - 1, seqs, 256), F32),
            *[pltpu.VMEM((layers, nd - 1, seqs, n), BF16) for n in sizes],
            pltpu.VMEM((layers, nd, seqs, width), BF16),
            pltpu.VMEM((layers, nt, rows, dloc), BF16),
            pltpu.VMEM((layers, nt - 1, rows, dloc), BF16),
            pltpu.VMEM((layers, nt, rows, dloc), BF16),
            pltpu.VMEM((batch, dloc), BF16),
            pltpu.VMEM((seqs, keys), F32),
            pltpu.VMEM((seqs, width), F32),
            dma((layers, 6)),
            dma((layers,)),
            dma((layers, 5, nd - 1)),
            dma((layers, 5, nd - 1)),
            dma((layers, nd - 1)),
            dma((layers, nd - 1)),
            dma((layers, nt - 1)),
            dma((layers, nt - 1)),
            dma((layers, nt - 1)),
            dma((layers, nt - 1)),
        ],
        compiler_params=pltpu.CompilerParams(
            collective_id=0, has_side_effects=True, vmem_limit_bytes=56 * 1024 * 1024
        ),
    )(
        tokens.reshape(nt, rows, dloc), lengths[:, None], norm_gain, dt_bias, a_log, d_skip,
        out_gain, conv_weight, conv_state.reshape(layers, seqs, (CONV_W - 1) * conv_w),
        w_z, w_x, w_b, w_c, w_dt, w_out, ssm_state,
    )
    offsets = jnp.arange(1, CONV_W - 1, dtype=jnp.int32)
    alive = lengths[:, None] + offsets[None, :] >= CONV_W
    kept = jnp.where(alive[None, :, :, None], conv_state[:, :, 1:], jnp.zeros((), BF16))
    conv_new = jnp.concatenate([kept, current[:, :, None]], axis=2)
    step = 2
    block = (1, step) + ssm_state.shape[2:]
    ssm_new = pl.pallas_call(
        state_kernel,
        grid=(layers, seqs // step),
        out_shape=jax.ShapeDtypeStruct(ssm_state.shape, F32),
        in_specs=[vmem, vmem, vmem, pl.BlockSpec(block, lambda l, s: (l, s, 0, 0, 0))],
        out_specs=pl.BlockSpec(block, lambda l, s: (l, s, 0, 0, 0)),
    )(dec, sx, wk, ssm_state)
    return stream.reshape(batch, dloc), conv_new, ssm_new


def solution(mesh):
    placed = (
        P("grp", "dp"),
        P(("grp", "dp")),
        P(None, "dp"),
        P(None, "dp", "tp"),
        P(None, "dp", "tp"),
        P(None, "dp", "tp"),
        P(None, "dp", "tp"),
        P(None, "dp", None),
        P(None, None, "tp"),
        P(None, "tp"),
        P(None, "tp"),
        P(None, "tp"),
        P(None, "tp"),
        P(None, "tp", "dp"),
        P(None, ("grp", "dp"), None, "tp"),
        P(None, ("grp", "dp"), "tp", None, None),
    )
    return jax.shard_map(
        functools.partial(body, mesh.shape["dp"], mesh.shape["tp"]),
        mesh=mesh,
        in_specs=placed,
        out_specs=(
            P("grp", "dp"),
            P(None, ("grp", "dp"), None, "tp"),
            P(None, ("grp", "dp"), "tp", None, None),
        ),
        check_vma=False,
    )
```

time: 391 us -> 82.7 us (0.21)
  waiting for transfers between devices: 198 us -> 0 us
  Pallas kernels: 0 us -> 72.1 us
  matrix products: 71.4 us -> 0 us
  blocking collectives: 51.6 us -> 0 us
  other arithmetic: 38.5 us -> 3.46 us
  between operations: 15.3 us -> 0.65 us
  local copies, waits for them, and re-layouts: 13.7 us -> 5.71 us
    reduce_scatter x12 -> x0, waiting for transfers between devices: 198 us -> none  [the longest x2 45.5 us: body(): lax.psum_scatter(part_z, 'dp', scatter_dimension=0, tiled=True)]
    pallas_call x0 -> x2, Pallas kernels: none -> 72.1 us  [the longest x1 49.6 us: body(): pl.pallas_call(functools.partial(block_kernel, nd, nt), out_shape=(jax.Sh...]
    dot_general x14 -> x0, matrix products: 71.4 us -> none  [the longest x2 43.2 us: body(): jnp.einsum('bghpn,bgn->bghp', state_next, read_keys, precision=lax.Precis...]
    all_gather x4 -> x0, blocking collectives: 37.6 us -> none  [the longest x2 26.7 us: body(): lax.all_gather((own_rows + share).astype(jnp.bfloat16), 'tp', axis=0, til...]
    add x1, other arithmetic: 16.4 us -> 0.01 us  [body(): offsets = jnp.arange(1, CONV_W - 1, dtype=jnp.int32)]
    unnamed x2 -> x0, blocking collectives: 14 us -> none
    another operation x4 -> x0, other arithmetic: 12.8 us -> none  [body(): return (stream, jnp.stack(conv_list), jnp.stack(ssm_list))]
    slice x10 -> x0, local copies, waits for them, and re-layouts: 9.37 us -> none  [the longest x1 8.47 us: body(): ssm_state[layer_at]]
  transfers between devices with their start and end apart: 12 -> 0, of which waited for: 11 -> 0; matrix products, arithmetic and copies ran while one was open for 12% -> 0% of each run, Pallas kernels for 0% -> 0%
where the time goes in v1:
time: 82.7 us; the launch traced here: 81.9 us
  Pallas kernels  72.1 us (87%)
  local copies, waits for them, and re-layouts  5.71 us (7%)
  other arithmetic  3.46 us (4%)
    pallas_call x1, Pallas kernels, body(): pl.pallas_call(functools.partial(block_kernel, nd, nt), out_shape=(jax.Sh...  49.6 us
    pallas_call x1, Pallas kernels, body(): pl.pallas_call(state_kernel, grid=(layers, seqs // step), out_shape=jax.S...  22.5 us
    unnamed x4, local copies, waits for them, and re-layouts  2.61 us
    reshape x1, local copies, waits for them, and re-layouts, body(): conv_state.reshape(layers, seqs, (CONV_W - 1) * conv_w)  1.77 us
    concatenate x1, other arithmetic, body(): conv_new = jnp.concatenate([kept, current[:, :, None]], axis=2)  1.69 us

profile of v1, /device:TPU:0, one launch (start us, length us, event | category | flops | bytes accessed | tf_op | source)
XLA Modules:
  0.0 81.9 jit_solution(7960445788373403550)
XLA Ops:
  0.6 0.7 add_compare_fusion
  1.4 1.3 %copy.24.lens_ref = s32[16,1]{1,0:T(8,128)} copy(s32[16,1]{0,1:T(1,128)} %bitcast.13) | data formatting | bytes 128 | tf_op jit(solution)/shard_map/broadcast_in_dim | solution.py:395
  2.7 1.0 %slice_select_fusion = bf16[2,16,2,2048]{3,1,2,0:T(8,128)(2,1)S(1)} fusion(bf16[2,16,3,2048]{3,1,2,0:T(8,128)(2,1)} %param.30, pred[16,2]{0,1:T(4,128)(4,1)S(1)} %add_compare_fusion), kind=kLoop, calls=%fused_computation.1 | loop fusion | flops 131072 | bytes 524320 | tf_op jit(solution)/shard_map/jit(_where)/select_n | solution.py:401
  3.7 1.8 %copy.27 = bf16[2,3,2,8,2048]{4,3,1,2,0:T(8,128)(2,1)} copy(bf16[2,3,2,8,2048]{4,3,2,1,0:T(8,128)(2,1)} %bitcast.9) | data formatting | bytes 786432 | tf_op jit(solution)/shard_map/reshape | solution.py:396
  5.5 2.0 %copy.25.wdt_hbm = bf16[2,1024,64]{2,1,0:T(8,128)(2,1)} copy(bf16[2,1024,64]{1,2,0:T(8,128)(2,1)} %param.23) | data formatting | bytes 524288 | tf_op args[7]
  7.5 49.6 %shard_map.175 = (bf16[4,16,1024]{2,1,0:T(8,128)(2,1)}, bf16[2,16,2048]{2,1,0:T(8,128)(2,1)}, f32[2,16,1024]{2,1,0:T(8,128)}, f32[2,16,1024]{2,1,0:T(8,128)}, f32[2,16,512]{2,1,0:T(8,128)}) custom-call(bf16[4,16,1024]{2,1,0:T(8,128)(2,1)} %bitcast.10, s32[16,1]{1,0:T(8,128)} %copy.24.lens_ref, f32[2,1024]{1,0:T(2,128)} %gain_ref.1, f32[2,16]{1,0:T(2,128)} %bias_ref.1, ...), custom_call_target="tpu_custom_call" | custom-call | tf_op jit(solution)/shard_map/pallas_call | solution.py:350
  57.0 1.7 %pad_maximum_fusion = bf16[2,16,3,2048]{3,1,2,0:T(8,128)(2,1)} fusion(bf16[2,16,1,2048]{3,1,2,0:T(8,128)(2,1)} %bitcast.12, bf16[2,16,2,2048]{3,1,2,0:T(8,128)(2,1)S(1)} %slice_select_fusion), kind=kLoop, calls=%fused_computation | loop fusion | flops 196608 | bytes 786432 | tf_op jit(solution)/shard_map/concatenate | solution.py:402
  58.7 0.0 copy-start
  58.7 22.5 %shard_map.176 = f32[2,16,16,64,128]{4,3,2,1,0:T(8,128)} custom-call(f32[2,16,1024]{2,1,0:T(8,128)} %get-tuple-element.10.dec_ref, f32[2,16,1024]{2,1,0:T(8,128)} %get-tuple-element.11.sx_ref, f32[2,16,512]{2,1,0:T(8,128)} %get-tuple-element.12.wk_ref, f32[2,16,16,64,128]{4,3,2,1,0:T(8,128)} %state_ref.1), custom_call_target="tpu_custom_call" | custom-call | tf_op jit(solution)/shard_map/pallas_call | solution.py:405
  81.3 0.0 copy-done
  81.3 0.7 copy.29
  (1 shorter events, 0.0 us)
Async XLA Ops:
  58.7 22.5 %copy-start = (bf16[4,16,1024]{2,1,0:T(8,128)(2,1)S(1)}, bf16[4,16,1024]{2,1,0:T(8,128)(2,1)}, u32[]{:S(2)}) copy-start(bf16[4,16,1024]{2,1,0:T(8,128)(2,1)} %get-tuple-element.8) | copy-start | bytes 393220

commit v2 on v1

--- a/solution.py
+++ b/solution.py
@@ -30,7 +30,7 @@
     nd, nt,
     tokens_ref, lens_ref, gain_ref, bias_ref, alog_ref, skip_ref, ogain_ref, taps_ref, conv_ref,
     wz_hbm, wx_hbm, wb_hbm, wc_hbm, wdt_hbm, wo_hbm, state_hbm,
-    out_ref, cur_ref, dec_ref, sx_ref, wk_ref,
+    out_ref, cur_ref, kept_ref, dec_ref, sx_ref, wk_ref,
     wz, wx, wb, wc, wdt, wo, state,
     snd_e, snd_x, snd_b, snd_c, snd_z,
     rcv_e, rcv_x, rcv_b, rcv_c, rcv_z,
@@ -40,7 +40,7 @@
     dp = lax.axis_index("dp")
     tp = lax.axis_index("tp")
     layers = gain_ref.shape[0]
-    seqs = lens_ref.shape[0]
+    seqs = lens_ref.shape[1]
     batch = nd * seqs
     rows = batch // nt
     dloc = gain_ref.shape[1]
@@ -94,7 +94,7 @@
             total = total + rcv[layer, k].astype(F32)
         return total
 
-    heads_all = wdt.shape[2]
+    heads_all = wdt.shape[1]
     lheads = bias_ref.shape[1]
 
     def expand(values, offset):
@@ -109,7 +109,11 @@
     bias = expand(bias_ref[...], 0)
     rate = jnp.exp(expand(alog_ref[...], 0))
     skip = expand(skip_ref[...], 0)
-    lens = lens_ref[...]
+    spread = jnp.broadcast_to(lens_ref[...].astype(F32), (seqs, seqs))
+    diagonal = lax.broadcasted_iota(jnp.int32, (seqs, seqs), 0) == lax.broadcasted_iota(
+        jnp.int32, (seqs, seqs), 1
+    )
+    lens = jnp.sum(jnp.where(diagonal, spread, 0.0), axis=1, keepdims=True)
     pending = []
 
     for layer in range(layers):
@@ -133,7 +137,9 @@
             lax.fori_loop(0, n // tile, step, 0)
 
         weight(layer, 0).wait()
-        part_dt = jnp.dot(normed_s[...], wdt[layer], preferred_element_type=F32)
+        part_dt = lax.dot_general(
+            normed_s[...], wdt[layer], (((1,), (1,)), ((), ())), preferred_element_type=F32
+        )
         snd_e[layer, :, :, 0:128] = jnp.zeros((nd, seqs, 128), F32)
         snd_e[layer, :, :, 0:heads_all] = part_dt.reshape(nd, seqs, heads_all)
         snd_e[layer, :, :, 128:256] = jnp.broadcast_to(squares, (batch, 128)).reshape(
@@ -178,13 +184,14 @@
             pieces.append(reads[:, g * STATE : (g + 1) * STATE])
         current = jnp.concatenate(pieces, axis=1)
         cur_ref[layer] = current
-        conv_w = lgroups * GROUP_W
         summed = current.astype(F32) * taps_ref[
             layer, CONV_W - 1 : CONV_W, :
         ].astype(F32)
         for tap in range(CONV_W - 1):
-            past = conv_ref[layer, :, tap * conv_w : (tap + 1) * conv_w].astype(F32)
-            past = jnp.where(lens + tap >= CONV_W, past, 0.0)
+            past = conv_ref[layer, tap].astype(F32)
+            past = jnp.where(lens >= CONV_W - tap, past, 0.0)
+            if tap >= 1:
+                kept_ref[layer, tap - 1] = past.astype(BF16)
             summed = summed + past * taps_ref[layer, tap : tap + 1, :].astype(F32)
         active = silu(summed)
         head_in = jnp.concatenate(
@@ -300,7 +307,15 @@
         copy.wait_send()
 
 
-def state_kernel(dec_ref, sx_ref, wk_ref, state_ref, new_ref):
+def state_kernel(
+    stream_ref, cur_ref, kept_ref, dec_ref, sx_ref, wk_ref, state_ref, out_ref, conv_ref, new_ref
+):
+    @pl.when(jnp.logical_and(pl.program_id(0) == 0, pl.program_id(1) == 0))
+    def small():
+        out_ref[...] = stream_ref[...]
+        conv_ref[:, 0 : CONV_W - 2] = kept_ref[...]
+        conv_ref[:, CONV_W - 2] = cur_ref[...]
+
     count = state_ref.shape[1]
     first = pl.program_id(1) * count
     width = dec_ref.shape[2]
@@ -341,29 +356,30 @@
     rows = batch // nt
     width = w_x.shape[2]
     keys = w_b.shape[2]
-    heads_all = w_dt.shape[2]
+    turned = jnp.swapaxes(w_dt, 1, 2)
     conv_w = conv_weight.shape[2]
     vmem = pl.BlockSpec(memory_space=pltpu.VMEM)
     anywhere = pl.BlockSpec(memory_space=pl.ANY)
     dma = pltpu.SemaphoreType.DMA
     sizes = (width, keys, keys, width)
-    stream, current, dec, sx, wk = pl.pallas_call(
+    stream, current, kept, dec, sx, wk = pl.pallas_call(
         functools.partial(block_kernel, nd, nt),
         out_shape=(
             jax.ShapeDtypeStruct((nt, rows, dloc), BF16),
             jax.ShapeDtypeStruct((layers, seqs, conv_w), BF16),
+            jax.ShapeDtypeStruct((layers, CONV_W - 2, seqs, conv_w), BF16),
             jax.ShapeDtypeStruct((layers, seqs, width), F32),
             jax.ShapeDtypeStruct((layers, seqs, width), F32),
             jax.ShapeDtypeStruct((layers, seqs, keys), F32),
         ),
         in_specs=[vmem] * 9 + [anywhere] * 7,
-        out_specs=[vmem] * 5,
+        out_specs=[vmem] * 6,
         scratch_shapes=[
             pltpu.VMEM(w_z.shape, BF16),
             pltpu.VMEM(w_x.shape, BF16),
             pltpu.VMEM(w_b.shape, BF16),
             pltpu.VMEM(w_c.shape, BF16),
-            pltpu.VMEM(w_dt.shape, BF16),
+            pltpu.VMEM(turned.shape, BF16),
             pltpu.VMEM(w_out.shape, BF16),
             pltpu.VMEM(ssm_state.shape, F32),
             pltpu.VMEM((layers, nd, seqs, 256), F32),
@@ -392,24 +408,24 @@
             collective_id=0, has_side_effects=True, vmem_limit_bytes=56 * 1024 * 1024
         ),
     )(
-        tokens.reshape(nt, rows, dloc), lengths[:, None], norm_gain, dt_bias, a_log, d_skip,
-        out_gain, conv_weight, conv_state.reshape(layers, seqs, (CONV_W - 1) * conv_w),
-        w_z, w_x, w_b, w_c, w_dt, w_out, ssm_state,
+        tokens.reshape(nt, rows, dloc), lengths[None, :], norm_gain, dt_bias, a_log, d_skip,
+        out_gain, conv_weight, jnp.transpose(conv_state, (0, 2, 1, 3)),
+        w_z, w_x, w_b, w_c, turned, w_out, ssm_state,
     )
-    offsets = jnp.arange(1, CONV_W - 1, dtype=jnp.int32)
-    alive = lengths[:, None] + offsets[None, :] >= CONV_W
-    kept = jnp.where(alive[None, :, :, None], conv_state[:, :, 1:], jnp.zeros((), BF16))
-    conv_new = jnp.concatenate([kept, current[:, :, None]], axis=2)
     step = 2
     block = (1, step) + ssm_state.shape[2:]
-    ssm_new = pl.pallas_call(
+    mixed_out, conv_new, ssm_new = pl.pallas_call(
         state_kernel,
         grid=(layers, seqs // step),
-        out_shape=jax.ShapeDtypeStruct(ssm_state.shape, F32),
-        in_specs=[vmem, vmem, vmem, pl.BlockSpec(block, lambda l, s: (l, s, 0, 0, 0))],
-        out_specs=pl.BlockSpec(block, lambda l, s: (l, s, 0, 0, 0)),
-    )(dec, sx, wk, ssm_state)
-    return stream.reshape(batch, dloc), conv_new, ssm_new
+        out_shape=(
+            jax.ShapeDtypeStruct(stream.shape, BF16),
+            jax.ShapeDtypeStruct((layers, CONV_W - 1, seqs, conv_w), BF16),
+            jax.ShapeDtypeStruct(ssm_state.shape, F32),
+        ),
+        in_specs=[vmem] * 6 + [pl.BlockSpec(block, lambda l, s: (l, s, 0, 0, 0))],
+        out_specs=(vmem, vmem, pl.BlockSpec(block, lambda l, s: (l, s, 0, 0, 0))),
+    )(stream, current, kept, dec, sx, wk, ssm_state)
+    return mixed_out.reshape(batch, dloc), jnp.transpose(conv_new, (0, 2, 1, 3)), ssm_new
 
 
 def solution(mesh):

time: 82.7 us -> 73.7 us (0.89)
  local copies, waits for them, and re-layouts: 5.71 us -> 0 us
  other arithmetic: 3.46 us -> 0 us
    unnamed x4 -> x0, local copies, waits for them, and re-layouts: 2.61 us -> none
    reshape x1 -> x0, local copies, waits for them, and re-layouts: 1.77 us -> none  [body(): conv_state.reshape(layers, seqs, (CONV_W - 1) * conv_w)]
    concatenate x1 -> x0, other arithmetic: 1.69 us -> none  [body(): conv_new = jnp.concatenate([kept, current[:, :, None]], axis=2)]
    broadcast_in_dim x1 -> x0, local copies, waits for them, and re-layouts: 1.33 us -> none  [body(): lengths[:, None]]
    select_n x1 -> x0, other arithmetic: 1.04 us -> none  [body(): jnp.where(alive[None, :, :, None], conv_state[:, :, 1:], jnp.zeros((), BF...]
where the time goes in v2:
time: 73.7 us; the launch traced here: 73.1 us
  Pallas kernels  72.4 us (98%)
    pallas_call x1, Pallas kernels, body(): pl.pallas_call(functools.partial(block_kernel, nd, nt), out_shape=(jax.Sh...  49.7 us
    pallas_call x1, Pallas kernels, body(): pl.pallas_call(state_kernel, grid=(layers, seqs // step), out_shape=(jax....  22.7 us

profile of v2, /device:TPU:0, one launch (start us, length us, event | category | flops | bytes accessed | tf_op | source)
XLA Modules:
  0.0 73.1 jit_solution(9126497184654725461)
XLA Ops:
  0.6 49.7 %shard_map.175 = (bf16[4,16,1024]{2,1,0:T(8,128)(2,1)}, bf16[2,16,2048]{2,1,0:T(8,128)(2,1)}, bf16[2,2,16,2048]{3,2,1,0:T(8,128)(2,1)}, f32[2,16,1024]{2,1,0:T(8...) custom-call(bf16[4,16,1024]{2,1,0:T(8,128)(2,1)} %bitcast.8, s32[1,16]{1,0:T(1,128)} %bitcast.9, ...), custom_call_target="tpu_custom_call" | custom-call | tf_op jit(solution)/shard_map/pallas_call | solution.py:365
  50.3 22.7 %shard_map.176 = (bf16[4,16,1024]{2,1,0:T(8,128)(2,1)}, bf16[2,3,16,2048]{3,2,1,0:T(8,128)(2,1)}, f32[2,16,16,64,128]{4,3,2,1,0:T(8,128)}) custom-call(bf16[4,16,1024]{2,1,0:T(8,128)(2,1)} %get-tuple-element.12.stream_ref, bf16[2,16,2048]{2,1,0:T(8,128)(2,1)} %get-tuple-element.13.cur_ref, bf16[2,2,16,2048]{3,2,1,0:T(8,128)(2,1)} %get-tuple-element.14.kept_ref, ...), custom_call_target="tpu_custom_call" | custom-call | tf_op jit(solution)/shard_map/pallas_call | solution.py:417
